TPU v7x, 32 devices: a whole 2x2x4 slice. The times are simulated.
32 devices in a mesh: fs: 16 (over z, y, core), tp: 2 (over x).
Axes of the slice: x: 2, y: 2, z: 4, core: 2. Of those that a mesh axis runs over, the one named last changes fastest.
Arguments:
- tokens: bfloat16 [8192, 2048], P('fs', 'tp'), may hold values from -6 to 6
- norm_gain: float32 [2048], P('fs'), may hold values from 0.1 to 1.9
- up_trained: float32 [2048, 4096], P('fs', 'tp'), may hold values from -0.125 to 0.125
- down_trained: float32 [4096, 2048], P('fs', 'tp'), may hold values from -0.09375 to 0.09375
Outputs:
- up_serving: bfloat16 [2048, 4096], P(None, 'tp')
- down_serving: bfloat16 [4096, 2048], P('tp')
- mixed: bfloat16 [8192, 2048], P('fs', 'tp')
All inputs are finite; a program needn't handle non-finite values.
Results may differ from a plain program's by a relative error of at most 0.013.
Values may be sent and summed in bfloat16 or wider, within the bound.
A program may use at most 128 MiB of HBM per device.

v0:
```python
import jax
import jax.numpy as jnp
from jax import lax
from jax.sharding import PartitionSpec as P


def per_device(tokens, norm_gain, up_trained, down_trained):
    up_piece = (norm_gain[:, None] * up_trained).astype(jnp.bfloat16)
    up_serving = lax.all_gather(up_piece, "fs", axis=0, tiled=True)
    down_piece = down_trained.astype(jnp.bfloat16)
    group_count = lax.axis_size("fs")
    pair_count = lax.axis_size("tp")
    sliver = down_piece.shape[1] // group_count
    flipped = down_piece.T
    narrow = lax.all_to_all(flipped, "fs", split_axis=0, concat_axis=1, tiled=True)
    regrouped = lax.all_to_all(narrow, "tp", split_axis=1, concat_axis=0, tiled=True)
    spread = lax.all_gather(regrouped, "fs", axis=0, tiled=True)
    block_width = spread.shape[1]
    ordered = spread.reshape(group_count, pair_count, sliver, block_width).transpose(1, 0, 2, 3)
    down_serving = ordered.reshape(pair_count * group_count * sliver, block_width).T
    features = lax.all_gather(tokens, "tp", axis=1, tiled=True)
    widened = features.astype(jnp.float32)
    scale = lax.rsqrt(jnp.mean(widened * widened, axis=-1, keepdims=True) + 1e-06)
    normed = (widened * scale).astype(jnp.bfloat16)
    preact = jnp.dot(normed, up_serving, preferred_element_type=jnp.float32)
    hidden = jnp.square(jnp.maximum(preact, 0.0)).astype(jnp.bfloat16)
    partial_out = jnp.dot(hidden, down_serving, preferred_element_type=jnp.float32)
    summed = lax.psum_scatter(
        partial_out.astype(jnp.bfloat16), "tp", scatter_dimension=1, tiled=True
    )
    return (up_serving, down_serving, summed)


def solution(mesh):
    placed = (P("fs", "tp"), P("fs"), P("fs", "tp"), P("fs", "tp"))
    return jax.shard_map(
        per_device,
        mesh=mesh,
        in_specs=placed,
        out_specs=(P(None, "tp"), P("tp", None), P("fs", "tp")),
        check_vma=False,
    )
```

profile of v0, /device:TPU:0, one launch (start us, length us, event | category | flops | bytes accessed | tf_op | source)
XLA Modules:
  0.0 264.8 jit_solution(10153047460143289739)
XLA Ops:
  7.2 0.0 copy-start.2
  7.2 0.0 copy-start.1
  7.2 0.0 all-gather.8.cloned.1.call-start
  7.2 0.7 all-gather.8.cloned.1.call-update
  7.9 0.0 all-gather.6.cloned.1.call-start
  8.0 1.4 copy.12
  9.4 21.5 %all_to_all.35 = bf16[16,64,256]{2,1,0:T(8,128)(2,1)S(1)} all-to-all(bf16[16,64,256]{2,1,0:T(8,128)(2,1)S(1)} %bitcast.23), channel_id=1, replica_groups=mesh['fs'=16,'tp'=2] {'fs'}, dimensions={0} | all-to-all | bytes 1048576 | tf_op jit(solution)/shard_map/all_to_all | solution.py:15
  30.9 0.3 copy.13
  31.2 0.1 all_to_all.29
  31.3 0.2 copy.14
  31.5 17.9 %all_to_all.36 = bf16[64,2,2048]{2,0,1:T(8,128)(2,1)} all-to-all(bf16[64,2,2048]{2,0,1:T(8,128)(2,1)S(1)} %copy.14), channel_id=1, replica_groups=mesh['fs'=16,'tp'=2] {'tp'}, dimensions={1} | all-to-all | bytes 1048576 | tf_op jit(solution)/shard_map/all_to_all | solution.py:16
  49.4 0.0 all-gather.6.cloned.1.call-update
  49.4 0.0 all-gather.4.cloned.1.call-start
  49.4 0.0 copy-done.2
  49.4 0.0 copy-done.1
  49.5 0.9 multiply_convert_fusion.1
  50.4 0.0 all-gather.4.cloned.1.call-update
  50.4 0.0 reduce-scatter.2.cloned.1.call-start
  50.5 0.6 all-gather.8.cloned.1.call-done
  51.0 2.1 fusion
  53.1 74.4 %all-gather.6.cloned.1.call-done = bf16[2048,2048]{1,0:T(8,128)(2,1)} async-done(((bf16[128,2048]{1,0:T(8,128)(2,1)}), bf16[2048,2048]{1,0:T(8,128)(2,1)}) %all-gather.6.cloned.1.call-update) | async-done | bytes 8388624 | tf_op jit(solution)/shard_map/all_gather | solution.py:17
  127.5 0.0 copy-start
  127.5 8.6 %copy.15 = bf16[2,16,64,2048]{3,2,1,0:T(8,128)(2,1)} copy(bf16[2,16,64,2048]{3,2,0,1:T(8,128)(2,1)} %bitcast.22) | data formatting | bytes 16777216 | tf_op jit(solution)/shard_map/transpose | solution.py:19
  136.1 67.1 %all-gather.4.cloned.1.call-done = bf16[2048,2048]{1,0:T(8,128)(2,1)} async-done(((bf16[128,2048]{1,0:T(8,128)(2,1)}), bf16[2048,2048]{1,0:T(8,128)(2,1)}) %all-gather.4.cloned.1.call-update) | async-done | bytes 8388624 | tf_op jit(solution)/shard_map/all_gather | solution.py:9
  203.1 0.0 copy-done
  203.2 16.0 %convolution_convert_fusion = bf16[512,2048]{1,0:T(8,128)(2,1)} fusion(bf16[2048,2048]{1,0:T(8,128)(2,1)} %bitcast.20, bf16[2048,2048]{1,0:T(8,128)(2,1)} %all-gather.4.cloned.1.call-done, bf16[512,2048]{1,0:T(8,128)(2,1)S(1)} %copy-done, f32[512]{0:T(512)S(1)} %add_rsqrt_fusion), kind=kOutput, calls=%fused_computation.5 | convolution fusion | flops 8597274624 | bytes 20973568 | tf_op jit(solution)/shard_map/dot_general | solution.py:27
  219.1 0.0 reduce-scatter.2.cloned.1.call-update
  219.2 11.9 %copy.16 = bf16[2048,2048]{1,0:T(8,128)(2,1)} copy(bf16[2048,2048]{0,1:T(8,128)(2,1)} %bitcast.21) | data formatting | bytes 16777216
  231.1 18.7 %reduce-scatter.2.cloned.1.call-done = bf16[512,1024]{1,0:T(8,128)(2,1)} async-done(((bf16[512,2048]{1,0:T(8,128)(2,1)}), bf16[512,1024]{1,0:T(8,128)(2,1)}) %reduce-scatter.2.cloned.1.call-update) | async-done | bytes 1048592 | tf_op jit(solution)/shard_map/reduce_scatter | solution.py:28
  249.8 8.4 %copy.18 = bf16[2048,2048]{1,0:T(8,128)(2,1)} copy(bf16[2048,2048]{1,0:T(8,128)(2,1)} %all-gather.4.cloned.1.call-done) | data formatting | bytes 16777216
  (1 shorter events, 0.0 us)
Async XLA Ops:
  7.2 42.3 %copy-start.2 = (f32[128]{0:T(128)S(1)}, f32[128]{0:T(128)}, u32[]{:S(2)}) copy-start(f32[128]{0:T(128)} %param.5) | copy-start | bytes 1540
  7.2 42.3 %copy-start.1 = (f32[128,2048]{1,0:T(8,128)S(1)}, f32[128,2048]{1,0:T(8,128)}, u32[]{:S(2)}) copy-start(f32[128,2048]{1,0:T(8,128)} %param.6) | copy-start | bytes 3145732
  7.2 43.8 %all-gather.8.cloned.1.call-start = ((), (), s32[]{:S(2)}) async-start(), calls=%async_computation.5 | async-start | bytes 3145728 | tf_op jit(solution)/shard_map/all_gather | solution.py:21
  7.9 119.6 %all-gather.6.cloned.1.call-start = ((), (), s32[]{:S(2)}) async-start(), calls=%async_computation.4 | async-start | bytes 8912896 | tf_op jit(solution)/shard_map/all_gather | solution.py:17
  49.4 153.8 %all-gather.4.cloned.1.call-start = ((), (), s32[]{:S(2)}) async-start(), calls=%async_computation.3 | async-start | bytes 8912896 | tf_op jit(solution)/shard_map/all_gather | solution.py:9
  50.4 199.4 %reduce-scatter.2.cloned.1.call-start = ((), (), s32[]{:S(2)}) async-start(), calls=%async_computation.6 | async-start | bytes 3145728 | tf_op jit(solution)/shard_map/reduce_scatter | solution.py:28
  127.5 75.7 %copy-start = (bf16[512,2048]{1,0:T(8,128)(2,1)S(1)}, bf16[512,2048]{1,0:T(8,128)(2,1)}, u32[]{:S(2)}) copy-start(bf16[512,2048]{1,0:T(8,128)(2,1)} %all-gather.8.cloned.1.call-done) | copy-start | bytes 6291460
Sparse Core Ops, SparseCore 0:
  9.5 41.4 all-gather.7
  53.2 74.2 all-gather.5
  130.2 72.8 all-gather.3
  219.3 30.4 reduce-scatter.1
where the time goes:
time: 265 us
  waiting for transfers between devices  161 us (61%)
  blocking collectives  39.4 us (15%)
  local copies, waits for them, and re-layouts  31 us (12%)
  matrix products  16 us (6%)
  between operations  13.8 us (5%)
  other arithmetic  3 us (1%)
    all_gather x1, waiting for transfers between devices, per_device(): spread = lax.all_gather(regrouped, 'fs', axis=0, tiled=True)  74.4 us
    all_gather x1, waiting for transfers between devices, per_device(): up_serving = lax.all_gather(up_piece, 'fs', axis=0, tiled=True)  67.1 us
    unnamed x9, local copies, waits for them, and re-layouts  21.8 us
    all_to_all x1, blocking collectives, per_device(): lax.all_to_all(flipped, 'fs', split_axis=0, concat_axis=1, tiled=True)  21.5 us
    reduce_scatter x1, waiting for transfers between devices, per_device(): lax.psum_scatter(partial_out.astype(jnp.bfloat16), 'tp', scatter_dimensio...  18.7 us
    all_to_all x1, blocking collectives, per_device(): lax.all_to_all(narrow, 'tp', split_axis=1, concat_axis=0, tiled=True)  17.9 us
    dot_general x1, matrix products, per_device(): jnp.dot(hidden, down_serving, preferred_element_type=jnp.float32)  16 us
    transpose x1, local copies, waits for them, and re-layouts, per_device(): spread.reshape(group_count, pair_count, sliver, block_width)  8.59 us
  transfers between devices with their start and end apart: 4, of which 4 were waited for; matrix products, arithmetic and copies ran while one was open for 10% of the time, Pallas kernels for 0%

commit v1 on v0

v1 whole, which is shorter than its diff:
```python
import functools

import jax
import jax.numpy as jnp
from jax import lax
from jax.experimental import pallas as pl
from jax.experimental.pallas import tpu as pltpu
from jax.sharding import PartitionSpec as P

BF = jnp.bfloat16
F32 = jnp.float32


def plain_device(tokens, norm_gain, up_trained, down_trained):
    up_piece = (norm_gain[:, None] * up_trained).astype(BF)
    up_serving = lax.all_gather(up_piece, "fs", axis=0, tiled=True)
    down_piece = down_trained.astype(BF)
    group_count = lax.axis_size("fs")
    pair_count = lax.axis_size("tp")
    sliver = down_piece.shape[1] // group_count
    flipped = down_piece.T
    narrow = lax.all_to_all(flipped, "fs", split_axis=0, concat_axis=1, tiled=True)
    regrouped = lax.all_to_all(narrow, "tp", split_axis=1, concat_axis=0, tiled=True)
    spread = lax.all_gather(regrouped, "fs", axis=0, tiled=True)
    block_width = spread.shape[1]
    ordered = spread.reshape(group_count, pair_count, sliver, block_width).transpose(1, 0, 2, 3)
    down_serving = ordered.reshape(pair_count * group_count * sliver, block_width).T
    features = lax.all_gather(tokens, "tp", axis=1, tiled=True)
    widened = features.astype(F32)
    scale = lax.rsqrt(jnp.mean(widened * widened, axis=-1, keepdims=True) + 1e-06)
    normed = (widened * scale).astype(BF)
    preact = jnp.dot(normed, up_serving, preferred_element_type=F32)
    hidden = jnp.square(jnp.maximum(preact, 0.0)).astype(BF)
    partial_out = jnp.dot(hidden, down_serving, preferred_element_type=F32)
    summed = lax.psum_scatter(partial_out.astype(BF), "tp", scatter_dimension=1, tiled=True)
    return (up_serving, down_serving, summed)


def grid_of(mesh):
    n_fs, n_tp = mesh.shape["fs"], mesh.shape["tp"]
    if n_tp != 2 or n_fs % 4:
        return None
    ny, nc = 2, 2
    nz = n_fs // (ny * nc)
    if nz % n_tp:
        return None
    base = mesh.devices[0, 0].coords
    for f in range(n_fs):
        for t in range(n_tp):
            d = mesh.devices[f, t]
            at = (t, (f // nc) % ny, f // (nc * ny))
            if tuple(a - b for a, b in zip(d.coords, base)) != at or d.core_on_chip != f % nc:
                return None
    return nz, ny


def kernel(nz, tok_ref, upp_ref, dnp_ref, up_out, dn_out, mix_ref,
           up, dn, tok_peer, normed, hidden, part_out, part_in,
           up_recv, dn_recv, up_send, dn_send, x_send, x_recv, out_sem):
    f = lax.axis_index("fs")
    x = lax.axis_index("tp")
    c = f % 2
    y = (f // 2) % 2
    z = f // 4
    zb = nz // 2
    ru = upp_ref.shape[0]
    rd = dnp_ref.shape[0]
    rows, half = tok_ref.shape
    width = up.shape[1]
    local_f = f - x * (2 * zb * 2)
    in_block = (z // zb) == x

    def fs_of(zz, yy, cc):
        return (zz * 2 + yy) * 2 + cc

    right = {"fs": fs_of(z + 1, y, c)}
    left = {"fs": fs_of(z - 1, y, c)}
    across = {"fs": fs_of(z, 1 - y, c)}
    partner = {"fs": fs_of(z, y, 1 - c)}
    peer = {"tp": 1 - x}
    dirs = {"r": (0, right, z + 1 < nz), "l": (1, left, z > 0), "y": (2, across, None), "p": (3, partner, None)}

    barrier = pltpu.get_barrier_semaphore()

    def greet(who):
        pl.semaphore_signal(barrier, inc=1, device_id=who, device_id_type=pl.DeviceIdType.MESH)

    for who in (across, partner, peer):
        greet(who)
    pl.when(z + 1 < nz)(lambda: greet(right))
    pl.when(z > 0)(lambda: greet(left))
    pl.semaphore_wait(barrier, 3 + (z + 1 < nz).astype(jnp.int32) + (z > 0).astype(jnp.int32))

    sends = []

    def both(a, b):
        if a is None:
            return b
        if b is None:
            return a
        return jnp.logical_and(a, b)

    def guarded(cond, fn):
        if cond is None:
            fn()
        else:
            pl.when(cond)(fn)

    def rcopy(src, dst, ssem, rsem, who):
        return pltpu.make_async_remote_copy(src_ref=src, dst_ref=dst, send_sem=ssem, recv_sem=rsem,
                                            device_id=who, device_id_type=pl.DeviceIdType.MESH)

    def send(cond, make):
        guarded(cond, lambda: make().start())
        sends.append((cond, make))

    def up_slot(p):
        return up.at[pl.ds(pl.multiple_of(p * ru, ru), ru)]

    def dn_slot(h, q):
        return dn.at[h, pl.ds(pl.multiple_of(q * rd, rd), rd)]

    def up_forward(p, names, cond=None, src=None):
        for name in names:
            k, who, there = dirs[name]
            send(both(cond, there),
                 lambda k=k, who=who: rcopy(up_slot(p) if src is None else src, up_slot(p),
                                            up_send.at[p * 4 + k], up_recv.at[p], who))

    def up_wait(p, cond=None):
        guarded(cond, lambda: rcopy(up_slot(p), up_slot(p), up_send.at[p * 4], up_recv.at[p], partner).wait_recv())

    def sides(s):
        if s == 0:
            return [(z, None, None)]
        return [(z - s, z - s >= 0, "r"), (z + s, z + s < nz, "l")]

    def up_z(s):
        for zz, cond, onward in sides(s):
            p = fs_of(zz, y, c)
            up_wait(p, cond)
            up_forward(p, (onward, "y", "p"), cond)

    def up_y(s):
        for zz, cond, _ in sides(s):
            p = fs_of(zz, 1 - y, c)
            up_wait(p, cond)
            up_forward(p, ("p",), cond)

    def up_p(s):
        for zz, cond, _ in sides(s):
            for yy in (y, 1 - y):
                up_wait(fs_of(zz, yy, 1 - c), cond)

    def dn_id(zz, yy, cc):
        return fs_of(zz - x * zb, yy, cc)

    def dn_cond(zz, cond):
        return both(cond, (zz // zb) == x)

    def dn_forward(h, q, names, cond, src=None):
        for name in names:
            k, who, there = dirs[name]
            send(both(cond, there),
                 lambda k=k, who=who: rcopy(dn_slot(h, q) if src is None else src, dn_slot(h, q),
                                            dn_send.at[h, q * 4 + k], dn_recv.at[h, q], who))

    def dn_wait(h, q, cond):
        guarded(cond, lambda: rcopy(dn_slot(h, q), dn_slot(h, q), dn_send.at[h, q * 4], dn_recv.at[h, q],
                                    partner).wait_recv())

    def dn_src(h):
        if h == 0:
            dn_wait(0, local_f, in_block)
            dn_forward(0, local_f, ("r", "l", "y", "p"), in_block)
        else:
            dn_forward(1, local_f, ("r", "l", "y", "p"), in_block, src=dnp_ref)

    def dn_z(h, s):
        for zz, cond, onward in sides(s):
            cond = dn_cond(zz, cond)
            q = dn_id(zz, y, c)
            dn_wait(h, q, cond)
            dn_forward(h, q, (onward, "y", "p"), cond)

    def dn_y(h, s):
        for zz, cond, _ in sides(s):
            cond = dn_cond(zz, cond)
            q = dn_id(zz, 1 - y, c)
            dn_wait(h, q, cond)
            dn_forward(h, q, ("p",), cond)

    def dn_p(h, s):
        for zz, cond, _ in sides(s):
            cond = dn_cond(zz, cond)
            for yy in (y, 1 - y):
                dn_wait(h, dn_id(zz, yy, 1 - c), cond)

    def tile(i, n):
        return pl.ds(pl.multiple_of(i * n, n), n)

    nt = min(256, half, width)
    rt = min(64, rows)
    reps = width // nt

    def norm():
        @pl.loop(0, rows // rt)
        def _(i):
            r = tile(i, rt)
            mine = tok_ref[r, :].astype(F32)
            other = tok_peer[r, :].astype(F32)
            total = jnp.sum(mine * mine, axis=-1, keepdims=True) + jnp.sum(other * other, axis=-1, keepdims=True)
            scale = lax.rsqrt(total / (2 * half) + 1e-06)
            normed[x, r, :] = (mine * scale).astype(BF)
            normed[1 - x, r, :] = (other * scale).astype(BF)

    def up_dot(lo, hi):
        @pl.loop(lo, hi)
        def _(i):
            cols = tile(i, nt)
            acc = jnp.dot(normed[0], up[pl.ds(0, half), cols], preferred_element_type=F32)
            acc = acc + jnp.dot(normed[1], up[pl.ds(half, half), cols], preferred_element_type=F32)
            hidden[:, cols] = jnp.square(jnp.maximum(acc, 0.0)).astype(BF)

    def dn_dot(h, dst, extra=None):
        @pl.loop(0, half // nt)
        def _(i):
            cols = tile(i, nt)
            acc = jnp.dot(hidden[...], dn[h, :, cols], preferred_element_type=F32).astype(BF)
            if extra is not None:
                acc = (acc.astype(F32) + extra[:, cols].astype(F32)).astype(BF)
            dst[:, cols] = acc

    cross = lambda: rcopy(dnp_ref, dn_slot(0, f - (1 - x) * (2 * zb * 2)), x_send.at[0],
                          dn_recv.at[0, f - (1 - x) * (2 * zb * 2)], peer)
    send(jnp.logical_not(in_block), cross)
    send_tok = lambda: rcopy(tok_ref, tok_peer, x_send.at[1], x_recv.at[0], peer)
    send(None, send_tok)
    up_forward(f, ("r", "l", "y", "p"), src=upp_ref)
    own_up = pltpu.make_async_copy(upp_ref, up_slot(f), out_sem.at[0])
    own_up.start()
    own_dn = lambda: pltpu.make_async_copy(dnp_ref, dn_slot(1, local_f), out_sem.at[1])
    pl.when(in_block)(lambda: own_dn().start())

    last = nz - 1
    up_z(1)
    dn_src(0)
    up_y(0)
    for s in range(2, nz):
        up_z(s)
        dn_z(0, s - 1)
    up_y(1)
    dn_src(1)
    for s in range(2, nz):
        up_y(s)
    dn_z(0, last)
    send_tok().wait_recv()
    norm()
    own_up.wait()
    for s in range(nz):
        up_p(s)
    up_store = pltpu.make_async_copy(up, up_out, out_sem.at[2])
    up_store.start()
    dn_y(0, 0)
    cuts = [reps * k // nz for k in range(nz + 1)]
    for s in range(nz):
        up_dot(cuts[s], cuts[s + 1])
        if s + 1 < nz:
            dn_z(1, s + 1)
            dn_y(0, s + 1)
    for s in range(nz):
        dn_p(0, s)

    def store_half(h, sem):
        off = (1 - x if h == 0 else x) * half
        return pltpu.make_async_copy(dn.at[h], dn_out.at[:, pl.ds(pl.multiple_of(off, half), half)], sem)

    dn_dot(0, part_out)
    store_half(0, out_sem.at[3]).start()
    dn_y(1, 0)
    send_part = lambda: rcopy(part_out, part_in, x_send.at[2], x_recv.at[1], peer)
    send(None, send_part)
    for s in range(1, nz):
        dn_y(1, s)
    pl.when(in_block)(lambda: own_dn().wait())
    for s in range(nz):
        dn_p(1, s)
    store_half(1, out_sem.at[4]).start()
    send_part().wait_recv()
    dn_dot(1, mix_ref, part_in)
    for cond, make in sends:
        guarded(cond, lambda make=make: make().wait_send())
    up_store.wait()
    store_half(0, out_sem.at[3]).wait()
    store_half(1, out_sem.at[4]).wait()


def grid_device(nz, tokens, norm_gain, up_trained, down_trained):
    up_piece = (norm_gain[:, None] * up_trained).astype(BF)
    down_piece = down_trained.astype(BF)
    n_fs, n_tp = lax.axis_size("fs"), lax.axis_size("tp")
    ru, width = up_piece.shape
    rd, half = down_piece.shape
    rows = tokens.shape[0]
    d_model, blk = ru * n_fs, n_fs // n_tp
    vmem = pl.BlockSpec(memory_space=pltpu.VMEM)
    hbm = pl.BlockSpec(memory_space=pl.ANY)
    flops = 2 * rows * width * d_model * 2
    return pl.pallas_call(
        functools.partial(kernel, nz),
        out_shape=(
            jax.ShapeDtypeStruct((d_model, width), BF),
            jax.ShapeDtypeStruct((rd * blk, half * n_tp), BF),
            jax.ShapeDtypeStruct((rows, half), BF),
        ),
        in_specs=[vmem, vmem, vmem],
        out_specs=(hbm, hbm, vmem),
        scratch_shapes=[
            pltpu.VMEM((d_model, width), BF),
            pltpu.VMEM((n_tp, rd * blk, half), BF),
            pltpu.VMEM((rows, half), BF),
            pltpu.VMEM((n_tp, rows, half), BF),
            pltpu.VMEM((rows, width), BF),
            pltpu.VMEM((rows, half), BF),
            pltpu.VMEM((rows, half), BF),
            pltpu.SemaphoreType.DMA((n_fs,)),
            pltpu.SemaphoreType.DMA((n_tp, blk)),
            pltpu.SemaphoreType.DMA((n_fs * 4,)),
            pltpu.SemaphoreType.DMA((n_tp, blk * 4)),
            pltpu.SemaphoreType.DMA((3,)),
            pltpu.SemaphoreType.DMA((2,)),
            pltpu.SemaphoreType.DMA((5,)),
        ],
        compiler_params=pltpu.CompilerParams(
            collective_id=0, has_side_effects=True, vmem_limit_bytes=56 * 2**20
        ),
        cost_estimate=pl.CostEstimate(flops=flops, bytes_accessed=2 * d_model * width * 2, transcendentals=0),
    )(tokens, up_piece, down_piece)


def solution(mesh):
    placed = (P("fs", "tp"), P("fs"), P("fs", "tp"), P("fs", "tp"))
    grid = grid_of(mesh)
    body = plain_device if grid is None else functools.partial(grid_device, grid[0])
    return jax.shard_map(
        body,
        mesh=mesh,
        in_specs=placed,
        out_specs=(P(None, "tp"), P("tp", None), P("fs", "tp")),
        check_vma=False,
    )
```

time: 265 us -> 154 us (0.58)
  waiting for transfers between devices: 161 us -> 0 us
  Pallas kernels: 0 us -> 131 us
  blocking collectives: 39.4 us -> 0 us
  matrix products: 16 us -> 0 us
  between operations: 13.8 us -> 0.64 us
  local copies, waits for them, and re-layouts: 31 us -> 17.9 us
    all_gather x3 -> x0, waiting for transfers between devices: 142 us -> none  [the longest x1 74.4 us: per_device(): spread = lax.all_gather(regrouped, 'fs', axis=0, tiled=True)]
    pallas_call x0 -> x1, Pallas kernels: none -> 131 us  [grid_device(): pl.pallas_call(functools.partial(kernel, nz), out_shape=(jax.ShapeDtypeSt...]
    all_to_all x2 -> x0, blocking collectives: 39.4 us -> none  [the longest x1 21.5 us: per_device(): lax.all_to_all(flipped, 'fs', split_axis=0, concat_axis=1, tiled=True)]
    reduce_scatter x1 -> x0, waiting for transfers between devices: 18.7 us -> none  [per_device(): lax.psum_scatter(partial_out.astype(jnp.bfloat16), 'tp', scatter_dimensio...]
    dot_general x1 -> x0, matrix products: 16 us -> none  [per_device(): jnp.dot(hidden, down_serving, preferred_element_type=jnp.float32)]
    transpose x1 -> x0, local copies, waits for them, and re-layouts: 8.59 us -> none  [per_device(): spread.reshape(group_count, pair_count, sliver, block_width)]
    unnamed x9 -> x5, local copies, waits for them, and re-layouts: 21.8 us -> 17.9 us
    convert_element_type x1 -> x2, other arithmetic: 0.92 us -> 4.24 us  [the longest x1 2.14 us: grid_device(): up_piece = (norm_gain[:, None] * up_trained).astype(BF)]
  transfers between devices with their start and end apart: 4 -> 0, of which waited for: 4 -> 0; matrix products, arithmetic and copies ran while one was open for 10% -> 0% of each run, Pallas kernels for 0% -> 0%
where the time goes in v1:
time: 154 us; the launch traced here: 153 us
  Pallas kernels  131 us (85%)
  local copies, waits for them, and re-layouts  17.9 us (12%)
  other arithmetic  4.24 us (3%)
    pallas_call x1, Pallas kernels, grid_device(): pl.pallas_call(functools.partial(kernel, nz), out_shape=(jax.ShapeDtypeSt...  131 us
    unnamed x5, local copies, waits for them, and re-layouts  17.9 us

profile of v1, /device:TPU:0, one launch (start us, length us, event | category | flops | bytes accessed | tf_op | source)
XLA Modules:
  0.0 153.5 jit_solution(8258061823447676347)
XLA Ops:
  0.6 2.1 %multiply_convert_fusion.upp_ref = bf16[128,2048]{1,0:T(8,128)(2,1)} fusion(f32[128,2048]{1,0:T(8,128)} %param.6, f32[128]{0:T(128)} %param.5), kind=kLoop, calls=%fused_computation | loop fusion | flops 524288 | bytes 1573376 | tf_op jit(solution)/shard_map/convert_element_type | solution.py:299
  2.8 2.1 %convert_element_type.7.dnp_ref = bf16[256,1024]{1,0:T(8,128)(2,1)} convert(f32[256,1024]{1,0:T(8,128)} %param.7) | non-fusion elementwise | flops 262144 | bytes 1572864 | tf_op jit(solution)/shard_map/convert_element_type | solution.py:300
  4.9 130.6 %shard_map.67 = (bf16[2048,2048]{1,0:T(8,128)(2,1)}, bf16[2048,2048]{1,0:T(8,128)(2,1)}, bf16[512,1024]{1,0:T(8,128)(2,1)}) custom-call(bf16[512,1024]{1,0:T(8,128)(2,1)} %tok_ref.1, bf16[128,2048]{1,0:T(8,128)(2,1)} %multiply_convert_fusion.upp_ref, bf16[256,1024]{1,0:T(8,128)(2,1)} %convert_element_type.7.dnp_ref), custom_call_target="tpu_custom_call" | custom-call | flops 8589934592 | bytes 16777216 | tf_op jit(solution)/shard_map/pallas_call | solution.py:309
  135.5 8.4 %copy.10 = bf16[2048,2048]{1,0:T(8,128)(2,1)} copy(bf16[2048,2048]{1,0:T(8,128)(2,1)} %get-tuple-element.6) | data formatting | bytes 16777216
  144.0 0.0 copy-start
  144.0 8.5 %copy.11 = bf16[2048,2048]{1,0:T(8,128)(2,1)} copy(bf16[2048,2048]{1,0:T(8,128)(2,1)} %get-tuple-element.7) | data formatting | bytes 16777216
  152.5 0.0 copy-done
  152.5 1.0 copy.12
Async XLA Ops:
  144.0 8.5 %copy-start = (bf16[512,1024]{1,0:T(8,128)(2,1)S(1)}, bf16[512,1024]{1,0:T(8,128)(2,1)}, u32[]{:S(2)}) copy-start(bf16[512,1024]{1,0:T(8,128)(2,1)} %get-tuple-element.8) | copy-start | bytes 3145732

commit v2 on v1

v2 whole, which is shorter than its diff:
```python
import functools

import jax
import jax.numpy as jnp
from jax import lax
from jax.experimental import pallas as pl
from jax.experimental.pallas import tpu as pltpu
from jax.sharding import PartitionSpec as P

BF = jnp.bfloat16
F32 = jnp.float32


def plain_device(tokens, norm_gain, up_trained, down_trained):
    up_piece = (norm_gain[:, None] * up_trained).astype(BF)
    up_serving = lax.all_gather(up_piece, "fs", axis=0, tiled=True)
    down_piece = down_trained.astype(BF)
    group_count = lax.axis_size("fs")
    pair_count = lax.axis_size("tp")
    sliver = down_piece.shape[1] // group_count
    flipped = down_piece.T
    narrow = lax.all_to_all(flipped, "fs", split_axis=0, concat_axis=1, tiled=True)
    regrouped = lax.all_to_all(narrow, "tp", split_axis=1, concat_axis=0, tiled=True)
    spread = lax.all_gather(regrouped, "fs", axis=0, tiled=True)
    block_width = spread.shape[1]
    ordered = spread.reshape(group_count, pair_count, sliver, block_width).transpose(1, 0, 2, 3)
    down_serving = ordered.reshape(pair_count * group_count * sliver, block_width).T
    features = lax.all_gather(tokens, "tp", axis=1, tiled=True)
    widened = features.astype(F32)
    scale = lax.rsqrt(jnp.mean(widened * widened, axis=-1, keepdims=True) + 1e-06)
    normed = (widened * scale).astype(BF)
    preact = jnp.dot(normed, up_serving, preferred_element_type=F32)
    hidden = jnp.square(jnp.maximum(preact, 0.0)).astype(BF)
    partial_out = jnp.dot(hidden, down_serving, preferred_element_type=F32)
    summed = lax.psum_scatter(partial_out.astype(BF), "tp", scatter_dimension=1, tiled=True)
    return (up_serving, down_serving, summed)


def grid_of(mesh):
    n_fs, n_tp = mesh.shape["fs"], mesh.shape["tp"]
    if n_tp != 2 or n_fs % 4:
        return None
    ny, nc = 2, 2
    nz = n_fs // (ny * nc)
    if nz % n_tp:
        return None
    base = mesh.devices[0, 0].coords
    for f in range(n_fs):
        for t in range(n_tp):
            d = mesh.devices[f, t]
            at = (t, (f // nc) % ny, f // (nc * ny))
            if tuple(a - b for a, b in zip(d.coords, base)) != at or d.core_on_chip != f % nc:
                return None
    return nz, ny


PARTS = 2


def kernel(nz, tok_ref, gain_ref, upt_ref, dnt_ref, up, dn, hidden, part_in,
           dnp_ref, tok_peer, normed, part_out,
           up_recv, dn_recv, up_send, dn_send, x_send, x_recv, out_sem):
    f = lax.axis_index("fs")
    x = lax.axis_index("tp")
    c = f % 2
    y = (f // 2) % 2
    z = f // 4
    zb = nz // 2
    ru = upt_ref.shape[0]
    rd = dnp_ref.shape[0]
    su, sd = ru // PARTS, rd // PARTS
    rows, half = tok_ref.shape
    width = up.shape[1]
    local_f = f - x * (2 * zb * 2)
    in_block = (z // zb) == x

    def fs_of(zz, yy, cc):
        return (zz * 2 + yy) * 2 + cc

    right = {"fs": fs_of(z + 1, y, c)}
    left = {"fs": fs_of(z - 1, y, c)}
    across = {"fs": fs_of(z, 1 - y, c)}
    partner = {"fs": fs_of(z, y, 1 - c)}
    peer = {"tp": 1 - x}
    dirs = {"r": (0, right, z + 1 < nz), "l": (1, left, z > 0), "y": (2, across, None), "p": (3, partner, None)}

    lanes = 128
    spread = jnp.broadcast_to(gain_ref[...], (lanes, ru)).T

    @pl.loop(0, width // lanes)
    def _(i):
        cols = pl.ds(pl.multiple_of(i * lanes, lanes), lanes)
        up[pl.ds(pl.multiple_of(f * ru, ru), ru), cols] = (spread * upt_ref[:, cols]).astype(BF)

    @pl.loop(0, rd // 32)
    def _(i):
        r = pl.ds(pl.multiple_of(i * 32, 32), 32)
        dnp_ref[r, :] = dnt_ref[r, :].astype(BF)

    barrier = pltpu.get_barrier_semaphore()

    def greet(who):
        pl.semaphore_signal(barrier, inc=1, device_id=who, device_id_type=pl.DeviceIdType.MESH)

    for who in (across, partner, peer):
        greet(who)
    pl.when(z + 1 < nz)(lambda: greet(right))
    pl.when(z > 0)(lambda: greet(left))
    pl.semaphore_wait(barrier, 3 + (z + 1 < nz).astype(jnp.int32) + (z > 0).astype(jnp.int32))

    sends = []

    def both(a, b):
        if a is None:
            return b
        if b is None:
            return a
        return jnp.logical_and(a, b)

    def guarded(cond, fn):
        if cond is None:
            fn()
        else:
            pl.when(cond)(fn)

    def rcopy(src, dst, ssem, rsem, who):
        return pltpu.make_async_remote_copy(src_ref=src, dst_ref=dst, send_sem=ssem, recv_sem=rsem,
                                            device_id=who, device_id_type=pl.DeviceIdType.MESH)

    def send(cond, make):
        guarded(cond, lambda: make().start())
        sends.append((cond, make))

    def up_slot(p, k):
        return up.at[pl.ds(pl.multiple_of(p * ru + k * su, su), su)]

    def dn_slot(h, q, k):
        return dn.at[h, pl.ds(pl.multiple_of(q * rd + k * sd, sd), sd)]

    def dnp(k):
        return dnp_ref.at[pl.ds(k * sd, sd)]

    def up_forward(p, k, names, cond=None):
        for name in names:
            j, who, there = dirs[name]
            send(both(cond, there),
                 lambda j=j, who=who: rcopy(up_slot(p, k), up_slot(p, k), up_send.at[k, p * 4 + j],
                                            up_recv.at[k, p], who))

    def up_wait(p, k, cond=None):
        guarded(cond, lambda: rcopy(up_slot(p, k), up_slot(p, k), up_send.at[k, p * 4], up_recv.at[k, p],
                                    partner).wait_recv())

    def sides(s):
        if s == 0:
            return [(z, None, None)]
        return [(z - s, z - s >= 0, "r"), (z + s, z + s < nz, "l")]

    def each(s):
        return [(k, *side) for k in range(PARTS) for side in sides(s)]

    def up_z(s):
        for k, zz, cond, onward in each(s):
            p = fs_of(zz, y, c)
            up_wait(p, k, cond)
            up_forward(p, k, (onward, "y", "p"), cond)

    def up_y(s):
        for k, zz, cond, _ in each(s):
            p = fs_of(zz, 1 - y, c)
            up_wait(p, k, cond)
            up_forward(p, k, ("p",), cond)

    def up_p(s):
        for k, zz, cond, _ in each(s):
            for yy in (y, 1 - y):
                up_wait(fs_of(zz, yy, 1 - c), k, cond)

    def dn_id(zz, yy, cc):
        return fs_of(zz - x * zb, yy, cc)

    def dn_cond(zz, cond):
        return both(cond, (zz // zb) == x)

    def dn_forward(h, q, k, names, cond, src=None):
        for name in names:
            j, who, there = dirs[name]
            send(both(cond, there),
                 lambda j=j, who=who: rcopy(dn_slot(h, q, k) if src is None else src, dn_slot(h, q, k),
                                            dn_send.at[h, k, q * 4 + j], dn_recv.at[h, k, q], who))

    def dn_wait(h, q, k, cond):
        guarded(cond, lambda: rcopy(dn_slot(h, q, k), dn_slot(h, q, k), dn_send.at[h, k, q * 4],
                                    dn_recv.at[h, k, q], partner).wait_recv())

    def dn_src(h):
        for k in range(PARTS):
            if h == 0:
                dn_wait(0, local_f, k, in_block)
                dn_forward(0, local_f, k, ("r", "l", "y", "p"), in_block)
            else:
                dn_forward(1, local_f, k, ("r", "l", "y", "p"), in_block, src=dnp(k))

    def dn_z(h, s):
        for k, zz, cond, onward in each(s):
            cond = dn_cond(zz, cond)
            q = dn_id(zz, y, c)
            dn_wait(h, q, k, cond)
            dn_forward(h, q, k, (onward, "y", "p"), cond)

    def dn_y(h, s):
        for k, zz, cond, _ in each(s):
            cond = dn_cond(zz, cond)
            q = dn_id(zz, 1 - y, c)
            dn_wait(h, q, k, cond)
            dn_forward(h, q, k, ("p",), cond)

    def dn_p(h, s):
        for k, zz, cond, _ in each(s):
            cond = dn_cond(zz, cond)
            for yy in (y, 1 - y):
                dn_wait(h, dn_id(zz, yy, 1 - c), k, cond)

    def tile(i, n):
        return pl.ds(pl.multiple_of(i * n, n), n)

    nt = min(256, half, width)
    rt = min(64, rows)
    reps = width // nt

    def norm():
        @pl.loop(0, rows // rt)
        def _(i):
            r = tile(i, rt)
            mine = tok_ref[r, :].astype(F32)
            other = tok_peer[r, :].astype(F32)
            total = jnp.sum(mine * mine, axis=-1, keepdims=True) + jnp.sum(other * other, axis=-1, keepdims=True)
            scale = lax.rsqrt(total / (2 * half) + 1e-06)
            normed[x, r, :] = (mine * scale).astype(BF)
            normed[1 - x, r, :] = (other * scale).astype(BF)

    def up_dot(lo, hi):
        @pl.loop(lo, hi)
        def _(i):
            cols = tile(i, nt)
            acc = jnp.dot(normed[0], up[pl.ds(0, half), cols], preferred_element_type=F32)
            acc = acc + jnp.dot(normed[1], up[pl.ds(half, half), cols], preferred_element_type=F32)
            hidden[:, cols] = jnp.square(jnp.maximum(acc, 0.0)).astype(BF)

    def dn_dot(h, dst):
        @pl.loop(0, half // nt)
        def _(i):
            cols = tile(i, nt)
            dst[:, cols] = jnp.dot(hidden[...], dn[h, :, cols], preferred_element_type=F32).astype(BF)

    far_q = f - (1 - x) * (2 * zb * 2)
    for k in range(PARTS):
        send(jnp.logical_not(in_block),
             lambda k=k: rcopy(dnp(k), dn_slot(0, far_q, k), x_send.at[2 + k], dn_recv.at[0, k, far_q], peer))
    send_tok = lambda: rcopy(tok_ref, tok_peer, x_send.at[0], x_recv.at[0], peer)
    send(None, send_tok)
    for k in range(PARTS):
        up_forward(f, k, ("r", "l", "y", "p"))
    own_dn = lambda: pltpu.make_async_copy(dnp_ref, dn.at[1, pl.ds(pl.multiple_of(local_f * rd, rd), rd)],
                                           out_sem.at[0])
    pl.when(in_block)(lambda: own_dn().start())

    last = nz - 1
    up_z(1)
    dn_src(0)
    up_y(0)
    for s in range(2, nz):
        up_z(s)
        dn_z(0, s - 1)
    up_y(1)
    dn_src(1)
    for s in range(2, nz):
        up_y(s)
    dn_z(0, last)
    send_tok().wait_recv()
    norm()
    for s in range(nz):
        up_p(s)
    dn_y(0, 0)
    cuts = [reps * k // nz for k in range(nz + 1)]
    for s in range(nz):
        up_dot(cuts[s], cuts[s + 1])
        if s + 1 < nz:
            dn_z(1, s + 1)
            dn_y(0, s + 1)
    for s in range(nz):
        dn_p(0, s)

    dn_dot(0, part_out)
    dn_y(1, 0)
    send_part = lambda: rcopy(part_out, part_in, x_send.at[1], x_recv.at[1], peer)
    send(None, send_part)
    for s in range(1, nz):
        dn_y(1, s)
    pl.when(in_block)(lambda: own_dn().wait())
    for s in range(nz):
        dn_p(1, s)
    send_part().wait_recv()
    for cond, make in sends:
        guarded(cond, lambda make=make: make().wait_send())


def finish(up, dn, hidden, part_in, up_out, dn_out, mix_out, mix, sems):
    x = lax.axis_index("tp")
    half = dn.shape[2]
    n = sems.shape[1]
    ru, rd = up.shape[0] // n, dn.shape[1] // n
    off = [(1 - x) * half, x * half]
    copies = []
    for k in range(n):
        r = pl.ds(k * ru, ru)
        copies.append(pltpu.make_async_copy(up.at[r], up_out.at[r], sems.at[0, k]))
        r = pl.ds(k * rd, rd)
        for h in range(2):
            cols = pl.ds(pl.multiple_of(off[h], half), half)
            copies.append(pltpu.make_async_copy(dn.at[h, r], dn_out.at[r, cols], sems.at[1 + h, k]))
    for copy in copies:
        copy.start()
    nt = min(256, half)

    @pl.loop(0, half // nt)
    def _(i):
        cols = pl.ds(pl.multiple_of(i * nt, nt), nt)
        own = jnp.dot(hidden[...], dn[1, :, cols], preferred_element_type=F32).astype(BF)
        mix[:, cols] = (own.astype(F32) + part_in[:, cols].astype(F32)).astype(BF)

    last = pltpu.make_async_copy(mix, mix_out, sems.at[3, 0])
    last.start()
    for copy in copies:
        copy.wait()
    last.wait()


def grid_device(nz, tokens, norm_gain, up_trained, down_trained):
    n_fs, n_tp = lax.axis_size("fs"), lax.axis_size("tp")
    ru, width = up_trained.shape
    rd, half = down_trained.shape
    rows = tokens.shape[0]
    d_model, blk = ru * n_fs, n_fs // n_tp
    vmem = pl.BlockSpec(memory_space=pltpu.VMEM)
    hbm = pl.BlockSpec(memory_space=pl.ANY)
    flops = 2 * rows * width * d_model
    held = pl.pallas_call(
        functools.partial(kernel, nz),
        out_shape=(
            jax.ShapeDtypeStruct((d_model, width), BF),
            jax.ShapeDtypeStruct((n_tp, rd * blk, half), BF),
            jax.ShapeDtypeStruct((rows, width), BF),
            jax.ShapeDtypeStruct((rows, half), BF),
        ),
        in_specs=[vmem] * 4,
        out_specs=(vmem,) * 4,
        scratch_shapes=[
            pltpu.VMEM((rd, half), BF),
            pltpu.VMEM((rows, half), BF),
            pltpu.VMEM((n_tp, rows, half), BF),
            pltpu.VMEM((rows, half), BF),
            pltpu.SemaphoreType.DMA((PARTS, n_fs)),
            pltpu.SemaphoreType.DMA((n_tp, PARTS, blk)),
            pltpu.SemaphoreType.DMA((PARTS, n_fs * 4)),
            pltpu.SemaphoreType.DMA((n_tp, PARTS, blk * 4)),
            pltpu.SemaphoreType.DMA((2 + PARTS,)),
            pltpu.SemaphoreType.DMA((2,)),
            pltpu.SemaphoreType.DMA((1,)),
        ],
        compiler_params=pltpu.CompilerParams(
            collective_id=0, has_side_effects=True, vmem_limit_bytes=16 * 2**20
        ),
        cost_estimate=pl.CostEstimate(flops=flops, bytes_accessed=2 * d_model * width * 2, transcendentals=0),
    )(tokens, norm_gain.reshape(1, ru), up_trained, down_trained)
    return pl.pallas_call(
        finish,
        out_shape=(
            jax.ShapeDtypeStruct((d_model, width), BF),
            jax.ShapeDtypeStruct((rd * blk, half * n_tp), BF),
            jax.ShapeDtypeStruct((rows, half), BF),
        ),
        in_specs=[vmem] * 4,
        out_specs=(hbm,) * 3,
        scratch_shapes=[pltpu.VMEM((rows, half), BF), pltpu.SemaphoreType.DMA((4, 8))],
        compiler_params=pltpu.CompilerParams(vmem_limit_bytes=8 * 2**20),
        cost_estimate=pl.CostEstimate(flops=flops, bytes_accessed=2 * d_model * width * 2, transcendentals=0),
    )(*held)


def solution(mesh):
    placed = (P("fs", "tp"), P("fs"), P("fs", "tp"), P("fs", "tp"))
    grid = grid_of(mesh)
    body = plain_device if grid is None else functools.partial(grid_device, grid[0])
    return jax.shard_map(
        body,
        mesh=mesh,
        in_specs=placed,
        out_specs=(P(None, "tp"), P("tp", None), P("fs", "tp")),
        check_vma=False,
    )
```

time: 154 us -> 132 us (0.86)
  local copies, waits for them, and re-layouts: 17.9 us -> 4.32 us
  other arithmetic: 4.24 us -> 0 us
  Pallas kernels: 131 us -> 127 us
    unnamed x5 -> x8, local copies, waits for them, and re-layouts: 17.9 us -> 4.32 us
    pallas_call x1, Pallas kernels: 131 us -> 120 us  [grid_device(): pl.pallas_call(functools.partial(kernel, nz), out_shape=(jax.ShapeDtypeSt...]
    pallas_call x0 -> x1, Pallas kernels: none -> 6.42 us  [grid_device(): pl.pallas_call(finish, out_shape=(jax.ShapeDtypeStruct((d_model, width),...]
    convert_element_type x2 -> x0, other arithmetic: 4.24 us -> none  [the longest x1 2.14 us: grid_device(): up_piece = (norm_gain[:, None] * up_trained).astype(BF)]
where the time goes in v2:
time: 132 us
  Pallas kernels  127 us (96%)
  local copies, waits for them, and re-layouts  4.32 us (3%)
    pallas_call x1, Pallas kernels, grid_device(): pl.pallas_call(functools.partial(kernel, nz), out_shape=(jax.ShapeDtypeSt...  120 us
    pallas_call x1, Pallas kernels, grid_device(): pl.pallas_call(finish, out_shape=(jax.ShapeDtypeStruct((d_model, width),...  6.42 us
    unnamed x8, local copies, waits for them, and re-layouts  4.32 us

profile of v2, /device:TPU:0, one launch (start us, length us, event | category | flops | bytes accessed | tf_op | source)
XLA Modules:
  0.0 131.6 jit_solution(2376313016868234354)
XLA Ops:
  0.6 0.0 copy-start
  0.6 1.2 copy-done
  1.9 0.0 copy-start.1
  1.9 1.2 copy-done.1
  3.1 0.0 copy-start.2
  3.1 1.2 copy-done.2
  4.3 0.0 copy-start.3
  4.3 0.7 copy-done.3
  5.0 120.2 %shard_map.67 = (bf16[2048,2048]{1,0:T(8,128)(2,1)S(1)}, bf16[2,2048,1024]{2,1,0:T(8,128)(2,1)S(1)}, bf16[512,2048]{1,0:T(8,128)(2,1)S(1)}, bf16[512,1024]{1,0:T(8,128)(2,1)S(1)}) custom-call(bf16[512,1024]{1,0:T(8,128)(2,1)S(1)} %copy-done, f32[1,128]{1,0:T(1,128)S(1)} %bitcast.1, f32[128,2048]{1,0:T(8,128)S(1)} %copy-done.1, f32[256,1024]{1,0:T(8,128)S(1)} %copy-done.2), custom_call_target="tpu_custom_call" | custom-call | flops 4294967296 | bytes 16777216 | tf_op jit(solution)/shard_map/pallas_call | solution.py:348
  125.2 6.4 %shard_map.68 = (bf16[2048,2048]{1,0:T(8,128)(2,1)}, bf16[2048,2048]{1,0:T(8,128)(2,1)}, bf16[512,1024]{1,0:T(8,128)(2,1)}) custom-call(bf16[2048,2048]{1,0:T(8,128)(2,1)S(1)} %get-tuple-element.7.up, bf16[2,2048,1024]{2,1,0:T(8,128)(2,1)S(1)} %get-tuple-element.8.dn, bf16[512,2048]{1,0:T(8,128)(2,1)S(1)} %get-tuple-element.9.hidden, ...), custom_call_target="tpu_custom_call" | custom-call | flops 4294967296 | bytes 16777216 | tf_op jit(solution)/shard_map/pallas_call | solution.py:376
Async XLA Ops:
  0.6 1.2 copy-start
  1.9 1.2 copy-start.1
  3.1 1.2 copy-start.2
  4.3 0.7 copy-start.3

commit v3 on v2

--- a/solution.py
+++ b/solution.py
@@ -267,34 +267,38 @@
 
     last = nz - 1
     up_z(1)
-    dn_src(0)
     up_y(0)
     for s in range(2, nz):
         up_z(s)
-        dn_z(0, s - 1)
-    up_y(1)
-    dn_src(1)
-    for s in range(2, nz):
-        up_y(s)
-    dn_z(0, last)
+        if s == 2:
+            dn_src(0)
+        else:
+            dn_z(0, s - 2)
+        if s == last:
+            dn_src(1)
+        up_y(s - 1)
+    dn_z(0, last - 1)
+    up_y(last)
     send_tok().wait_recv()
     norm()
     for s in range(nz):
         up_p(s)
-    dn_y(0, 0)
     cuts = [reps * k // nz for k in range(nz + 1)]
+    up_dot(cuts[0], cuts[1])
+    dn_z(0, last)
+    for s in range(1, nz):
+        if s < last:
+            dn_z(1, s)
+        up_dot(cuts[s], cuts[s + 1])
     for s in range(nz):
-        up_dot(cuts[s], cuts[s + 1])
-        if s + 1 < nz:
-            dn_z(1, s + 1)
-            dn_y(0, s + 1)
+        dn_y(0, s)
     for s in range(nz):
         dn_p(0, s)
-
     dn_dot(0, part_out)
     dn_y(1, 0)
     send_part = lambda: rcopy(part_out, part_in, x_send.at[1], x_recv.at[1], peer)
     send(None, send_part)
+    dn_z(1, last)
     for s in range(1, nz):
         dn_y(1, s)
     pl.when(in_block)(lambda: own_dn().wait())

time: 132 us -> 123 us (0.932)
  Pallas kernels: 127 us -> 116 us
    pallas_call x1, Pallas kernels: 120 us -> 110 us  [grid_device(): pl.pallas_call(functools.partial(kernel, nz), out_shape=(jax.ShapeDtypeSt...]
where the time goes in v3:
time: 123 us; the launch traced here: 121 us
  Pallas kernels  116 us (94%)
  local copies, waits for them, and re-layouts  4.32 us (4%)
    pallas_call x1, Pallas kernels, grid_device(): pl.pallas_call(functools.partial(kernel, nz), out_shape=(jax.ShapeDtypeSt...  110 us
    pallas_call x1, Pallas kernels, grid_device(): pl.pallas_call(finish, out_shape=(jax.ShapeDtypeStruct((d_model, width),...  6.42 us
    unnamed x8, local copies, waits for them, and re-layouts  4.32 us

profile of v3, /device:TPU:0, one launch (start us, length us, event | category | flops | bytes accessed | tf_op | source)
XLA Modules:
  0.0 121.5 jit_solution(1911345504480210336)
XLA Ops:
  0.6 0.0 copy-start
  0.6 1.2 %copy-done = bf16[512,1024]{1,0:T(8,128)(2,1)S(1)} copy-done((bf16[512,1024]{1,0:T(8,128)(2,1)S(1)}, bf16[512,1024]{1,0:T(8,128)(2,1)}, u32[]{:S(2)}) %copy-start) | copy-done | bytes 1048600
  1.9 0.0 copy-start.1
  1.9 1.2 %copy-done.1 = f32[128,2048]{1,0:T(8,128)S(1)} copy-done((f32[128,2048]{1,0:T(8,128)S(1)}, f32[128,2048]{1,0:T(8,128)}, u32[]{:S(2)}) %copy-start.1) | copy-done | bytes 1048600
  3.1 0.0 copy-start.2
  3.1 1.2 %copy-done.2 = f32[256,1024]{1,0:T(8,128)S(1)} copy-done((f32[256,1024]{1,0:T(8,128)S(1)}, f32[256,1024]{1,0:T(8,128)}, u32[]{:S(2)}) %copy-start.2) | copy-done | bytes 1048600
  4.3 0.0 copy-start.3
  4.3 0.7 copy-done.3
  5.0 110.1 %shard_map.67 = (bf16[2048,2048]{1,0:T(8,128)(2,1)S(1)}, bf16[2,2048,1024]{2,1,0:T(8,128)(2,1)S(1)}, bf16[512,2048]{1,0:T(8,128)(2,1)S(1)}, bf16[512,1024]{1,0:T(8,128)(2,1)S(1)}) custom-call(bf16[512,1024]{1,0:T(8,128)(2,1)S(1)} %copy-done, f32[1,128]{1,0:T(1,128)S(1)} %bitcast.1, f32[128,2048]{1,0:T(8,128)S(1)} %copy-done.1, f32[256,1024]{1,0:T(8,128)S(1)} %copy-done.2), custom_call_target="tpu_custom_call" | custom-call | flops 4294967296 | bytes 16777216 | tf_op jit(solution)/shard_map/pallas_call | solution.py:352
  115.0 6.4 %shard_map.68 = (bf16[2048,2048]{1,0:T(8,128)(2,1)}, bf16[2048,2048]{1,0:T(8,128)(2,1)}, bf16[512,1024]{1,0:T(8,128)(2,1)}) custom-call(bf16[2048,2048]{1,0:T(8,128)(2,1)S(1)} %get-tuple-element.7.up, bf16[2,2048,1024]{2,1,0:T(8,128)(2,1)S(1)} %get-tuple-element.8.dn, bf16[512,2048]{1,0:T(8,128)(2,1)S(1)} %get-tuple-element.9.hidden, ...), custom_call_target="tpu_custom_call" | custom-call | flops 4294967296 | bytes 16777216 | tf_op jit(solution)/shard_map/pallas_call | solution.py:380
Async XLA Ops:
  0.6 1.2 %copy-start = (bf16[512,1024]{1,0:T(8,128)(2,1)S(1)}, bf16[512,1024]{1,0:T(8,128)(2,1)}, u32[]{:S(2)}) copy-start(bf16[512,1024]{1,0:T(8,128)(2,1)} %tok_ref.1) | copy-start | bytes 3145732
  1.9 1.2 %copy-start.1 = (f32[128,2048]{1,0:T(8,128)S(1)}, f32[128,2048]{1,0:T(8,128)}, u32[]{:S(2)}) copy-start(f32[128,2048]{1,0:T(8,128)} %upt_ref.1) | copy-start | bytes 3145732
  3.1 1.2 %copy-start.2 = (f32[256,1024]{1,0:T(8,128)S(1)}, f32[256,1024]{1,0:T(8,128)}, u32[]{:S(2)}) copy-start(f32[256,1024]{1,0:T(8,128)} %dnt_ref.1) | copy-start | bytes 3145732
  4.3 0.7 copy-start.3
